TPU v7x, 512 devices: a whole 4x8x8 slice. The times are simulated.
512 devices in a mesh: ep: 32 (over z, x), tp: 16 (over y, core).
Axes of the slice: x: 4, y: 8, z: 8, core: 2. Of those that a mesh axis runs over, the one named last changes fastest.
Arguments:
- tokens: bfloat16 [768, 4096], P('ep'), may hold values from -6 to 6
- norm_gain: float32 [4096], replicated, may hold values from 0.1 to 1.9
- routes: int32 [768, 6], P('ep'), may hold values from 0 to 63, all different within a row; in each aligned block of 24 rows (0 to 23, 24 to 47, ...) at most 6 rows name the same one
- route_scores: float32 [768, 6], P('ep'), may hold values from 0.05 to 1
- expert_gate: bfloat16 [64, 1024, 4096], P('ep', 'tp'), may hold values from -0.09375 to 0.09375
- expert_up: bfloat16 [64, 1024, 4096], P('ep', 'tp'), may hold values from -0.09375 to 0.09375
- expert_down: bfloat16 [64, 1024, 4096], P('ep', 'tp'), may hold values from -0.1875 to 0.1875
- shared_gate: bfloat16 [1024, 4096], P('tp'), may hold values from -0.09375 to 0.09375
- shared_up: bfloat16 [1024, 4096], P('tp'), may hold values from -0.09375 to 0.09375
- shared_down: bfloat16 [1024, 4096], P('tp'), may hold values from -0.1875 to 0.1875
Outputs:
- mixed: bfloat16 [768, 4096], P('ep', 'tp')
Inputs may be any that keep to these rules, and one draw needn't show every extreme that they name: `routes`: each row names 6 different experts. In the rows of one device (aligned blocks of 24 rows) no expert is named by more than 6 rows, and in some block one expert is named by exactly 6 rows.
All inputs are finite; a program needn't handle non-finite values.
Results may differ from a plain program's by a relative error of at most 0.02.
Values may be sent and summed in bfloat16 or wider, within the bound.
No kernel may reach another device: no remote copies, remote signals or barrier semaphores. Data moves between devices by JAX's collectives and lax.ppermute only.
A program may use at most 64 MiB of HBM per device.

v0:
```python
import jax
import jax.numpy as jnp
from jax import lax
from jax.sharding import PartitionSpec as P


def in_one_piece(arrays, axis, dim, along):
    widths = [a.shape[along] for a in arrays]
    both = jnp.concatenate(arrays, axis=along)
    filled = lax.psum_scatter(both, axis, scatter_dimension=dim, tiled=True)
    return tuple(jnp.split(filled, [sum(widths[:k]) for k in range(1, len(widths))], axis=along))


def capacity(tok_rows, chosen, experts):
    return min(tok_rows, max(4, 2 * ((tok_rows * chosen + experts - 1) // experts)))


def slot_index(route_block, experts, slot_count):
    flat = route_block.reshape(-1)
    onehot = (flat[:, None] == jnp.arange(experts, dtype=jnp.int32)[None, :]).astype(jnp.int32)
    before = jnp.cumsum(onehot, 0) - onehot
    order = jnp.sum(before * onehot, 1)
    return (flat * slot_count + order).reshape(route_block.shape)


def rounded(values):
    return lax.optimization_barrier(values.astype(jnp.bfloat16)).astype(jnp.float32)


def body(
    tokens,
    norm_gain,
    routes,
    route_scores,
    expert_gate,
    expert_up,
    expert_down,
    shared_gate,
    shared_up,
    shared_down,
):
    tok_rows, width = tokens.shape
    chosen = routes.shape[1]
    ep_size = lax.axis_size("ep")
    local = expert_gate.shape[0]
    experts = local * ep_size
    slot_count = capacity(tok_rows, chosen, experts)
    values = tokens.astype(jnp.float32)
    normed = (
        values * lax.rsqrt(jnp.mean(values * values, -1, keepdims=True) + 1e-06) * norm_gain
    ).astype(jnp.bfloat16)
    slots = slot_index(routes, experts, slot_count)
    tp_size = lax.axis_size("tp")
    columns = width // tp_size
    cells = jnp.arange(experts * slot_count, dtype=jnp.int32)
    table = jnp.sum((slots[None, :, :] == cells[:, None, None]).astype(jnp.float32), 2).astype(
        jnp.bfloat16
    )
    own_cols = lax.dynamic_slice_in_dim(normed, lax.axis_index("tp") * columns, columns, 1)
    buffer = jnp.dot(table, own_cols, preferred_element_type=jnp.float32).astype(jnp.bfloat16)
    buffer = buffer.reshape(ep_size, local, slot_count, columns)
    arrived = lax.all_to_all(buffer, "ep", split_axis=0, concat_axis=0, tiled=True)
    piece = lax.all_gather(arrived, "tp", axis=3, tiled=True)
    gate = jnp.einsum("secd,efd->secf", piece, expert_gate, preferred_element_type=jnp.float32)
    upper = jnp.einsum("secd,efd->secf", piece, expert_up, preferred_element_type=jnp.float32)
    gate, upper = (gate, upper)
    hidden = (jax.nn.silu(gate) * upper).astype(jnp.bfloat16)
    partial_value = rounded(
        jnp.einsum("secf,efd->secd", hidden, expert_down, preferred_element_type=jnp.float32)
    )
    shared_g = jnp.einsum("td,fd->tf", normed, shared_gate, preferred_element_type=jnp.float32)
    shared_u = jnp.einsum("td,fd->tf", normed, shared_up, preferred_element_type=jnp.float32)
    shared_hidden = (jax.nn.silu(shared_g) * shared_u).astype(jnp.bfloat16)
    shared_part = rounded(jnp.dot(shared_hidden, shared_down, preferred_element_type=jnp.float32))
    summed, shared_out = tuple(
        (
            part.astype(jnp.float32)
            for part in in_one_piece(
                (
                    partial_value.reshape(-1, width).astype(jnp.bfloat16),
                    shared_part.astype(jnp.bfloat16),
                ),
                "tp",
                1,
                0,
            )
        )
    )
    expert_out = summed.astype(jnp.bfloat16).reshape(ep_size, local * slot_count, -1)
    returned = lax.all_to_all(expert_out, "ep", split_axis=0, concat_axis=0, tiled=True).reshape(
        experts * slot_count, -1
    )
    weights = route_scores / jnp.sum(route_scores, -1, keepdims=True) * 2.5
    every_slot = jnp.arange(experts * slot_count, dtype=jnp.int32)
    combine = jnp.sum(
        weights[:, :, None] * (slots[:, :, None] == every_slot[None, None, :]).astype(jnp.float32),
        1,
    )
    routed = jnp.dot(combine, returned.astype(jnp.float32))
    return (shared_out + routed).astype(jnp.bfloat16)


def solution(mesh):
    in_specs = (
        P("ep", None),
        P(),
        P("ep", None),
        P("ep", None),
        P("ep", "tp", None),
        P("ep", "tp", None),
        P("ep", "tp", None),
        P("tp", None),
        P("tp", None),
        P("tp", None),
    )
    out_specs = P("ep", "tp")
    return jax.shard_map(body, mesh=mesh, in_specs=in_specs, out_specs=out_specs, check_vma=False)
```

profile of v0, /device:TPU:25, one launch (start us, length us, event | category | flops | bytes accessed | tf_op | source)
XLA Modules:
  0.0 199.0 jit_solution(11321514032493120497)
XLA Ops:
  6.6 0.9 copy.46
  7.5 0.1 eq.48
  7.6 0.6 reduce-window.6
  8.2 0.2 slice_reduce_fusion
  8.4 0.1 bitcast_bitcast_fusion
  8.6 0.1 reduce_sum.48
  8.7 0.1 copy.49
  8.8 0.7 multiply_add_fusion
  9.5 0.1 convert_reduce_fusion
  9.6 1.1 fusion.9
  10.6 1.1 fusion.11
  11.7 0.2 convolution_convert_fusion.2
  12.0 0.1 reshape.49
  12.0 0.2 copy.50
  12.2 22.7 %all_to_all.10 = bf16[32,2,6,256]{3,1,2,0:T(2,128)(2,1)S(1)} all-to-all(bf16[32,2,6,256]{3,1,2,0:T(2,128)(2,1)S(1)} %copy.50), channel_id=1, replica_groups=mesh['ep'=32,'tp'=16] {'ep'}, dimensions={0} | all-to-all | bytes 393216 | tf_op jit(solution)/shard_map/all_to_all | solution.py:62
  34.9 0.7 copy.51
  35.6 0.0 reduce-scatter.2.cloned.1.call-start
  35.6 0.2 fusion.31
  35.9 1.8 convolution_convert_fusion.1
  37.7 41.6 %all-gather.2.cloned.1.call-done = bf16[32,2,6,4096]{3,0,2,1:T(8,128)(2,1)} async-done(((bf16[32,2,6,256]{3,0,2,1:T(8,128)(2,1)}), bf16[32,2,6,4096]{3,0,2,1:T(8,128)(2,1)}) %all-gather.2.cloned.1.call-update) | async-done | bytes 3145744 | tf_op jit(solution)/shard_map/all_gather | solution.py:63
  79.3 2.8 %convolution_bitcast_fusion.1 = f32[32,2,6,64]{3,0,2,1:T(8,128)S(1)} fusion(bf16[32,2,6,4096]{3,0,2,1:T(8,128)(2,1)} %all-gather.2.cloned.1.call-done, bf16[2,64,4096]{2,1,0:T(8,128)(2,1)S(1)} %copy-done.1), kind=kOutput, calls=%fused_computation.7 | convolution fusion | flops 201326592 | bytes 4292608 | tf_op jit(solution)/shard_map/secd,efd->secf/dot_general | solution.py:64
  82.2 5.7 %fusion = bf16[32,2,6,4096]{3,0,2,1:T(8,128)(2,1)} fusion(bf16[32,2,6,4096]{3,0,2,1:T(8,128)(2,1)} %all-gather.2.cloned.1.call-done, bf16[2,64,4096]{2,1,0:T(8,128)(2,1)S(1)} %copy-done, bf16[2,64,4096]{2,1,0:T(8,128)(2,1)} %param.15, f32[32,2,6,64]{3,0,2,1:T(8,128)S(1)} %convolution_bitcast_fusion.1), kind=kOutput, calls=%fused_computation.1 | convolution fusion | flops 404373504 | bytes 8486912 | tf_op jit(solution)/shard_map/secf,efd->secd/dot_general | solution.py:69
  87.9 5.6 %copy.52 = bf16[32,2,6,4096]{3,2,1,0:T(8,128)(2,1)} copy(bf16[32,2,6,4096]{3,0,2,1:T(8,128)(2,1)} %fusion) | data formatting | bytes 6291456 | tf_op jit(solution)/shard_map/optimization_barrier | solution.py:27
  93.5 5.7 %convert_element_type.60 = bf16[384,4096]{1,0:T(8,128)(2,1)} reshape(bf16[32,2,6,4096]{3,2,1,0:T(8,128)(2,1)} %copy.52) | data formatting | bytes 6291456 | tf_op jit(solution)/shard_map/convert_element_type | solution.py:80
  99.2 3.9 %pad_maximum_fusion = bf16[408,4096]{1,0:T(8,128)(2,1)} fusion(bf16[24,4096]{1,0:T(8,128)(2,1)S(1)} %convolution_convert_fusion.1, bf16[384,4096]{1,0:T(8,128)(2,1)} %convert_element_type.60), kind=kLoop, calls=%fused_computation.3 | loop fusion | flops 6684672 | bytes 6684672 | tf_op jit(solution)/shard_map/concatenate | solution.py:9
  103.2 64.6 %reduce-scatter.2.cloned.1.call-done = bf16[408,256]{1,0:T(8,128)(2,1)} async-done(((bf16[408,4096]{1,0:T(8,128)(2,1)}), bf16[408,256]{1,0:T(8,128)(2,1)}) %reduce-scatter.2.cloned.1.call-update) | async-done | bytes 208912 | tf_op jit(solution)/shard_map/reduce_scatter | solution.py:10
  167.8 0.9 split.9
  168.7 0.7 reshape.50
  169.5 9.9 %all-to-all-start.1 = ((bf16[32,12,256]{2,1,0:T(8,128)(2,1)}), bf16[32,12,256]{2,1,0:T(8,128)(2,1)S(1)}, u32[]{:S(2)}, u32[]{:S(2)}) async-start(bf16[32,12,256]{2,1,0:T(8,128)(2,1)} %reshape.50), calls=%async_computation.2 | async-start | bytes 524288 | tf_op jit(solution)/shard_map/all_to_all | solution.py:90
  179.4 0.1 select_reduce_fusion
  179.5 11.1 %all-to-all-done.1 = bf16[32,12,256]{2,1,0:T(8,128)(2,1)S(1)} async-done(((bf16[32,12,256]{2,1,0:T(8,128)(2,1)}), bf16[32,12,256]{2,1,0:T(8,128)(2,1)S(1)}, u32[]{:S(2)}, u32[]{:S(2)}) %all-to-all-start.1) | async-done | bytes 196640 | tf_op jit(solution)/shard_map/all_to_all | solution.py:90
  190.7 1.5 fusion.3
  (20 shorter events, 0.2 us)
Async XLA Ops:
  6.5 75.6 %copy-start = (bf16[2,64,4096]{2,1,0:T(8,128)(2,1)S(1)}, bf16[2,64,4096]{2,1,0:T(8,128)(2,1)}, u32[]{:S(2)}) copy-start(bf16[2,64,4096]{2,1,0:T(8,128)(2,1)} %param.16) | copy-start | bytes 3145732
  6.5 29.1 %copy-start.2 = (bf16[64,4096]{1,0:T(8,128)(2,1)S(1)}, bf16[64,4096]{1,0:T(8,128)(2,1)}, u32[]{:S(2)}) copy-start(bf16[64,4096]{1,0:T(8,128)(2,1)} %param.17) | copy-start | bytes 1572868
  6.5 72.8 %copy-start.1 = (bf16[2,64,4096]{2,1,0:T(8,128)(2,1)S(1)}, bf16[2,64,4096]{2,1,0:T(8,128)(2,1)}, u32[]{:S(2)}) copy-start(bf16[2,64,4096]{2,1,0:T(8,128)(2,1)} %param.14) | copy-start | bytes 3145732
  6.5 72.8 %all-gather.2.cloned.1.call-start = ((), (), s32[]{:S(2)}) async-start(), calls=%async_computation.3 | async-start | bytes 3342336 | tf_op jit(solution)/shard_map/all_gather | solution.py:63
  35.6 132.2 %reduce-scatter.2.cloned.1.call-start = ((), (), s32[]{:S(2)}) async-start(), calls=%async_computation.4 | async-start | bytes 3551232 | tf_op jit(solution)/shard_map/reduce_scatter | solution.py:10
  103.1 76.3 %copy-start.3 = (f32[24,6]{0,1:T(8,128)S(1)}, f32[24,6]{0,1:T(8,128)}, u32[]{:S(2)}) copy-start(f32[24,6]{0,1:T(8,128)} %param.13) | copy-start | bytes 1732
  169.5 21.1 %all-to-all-start.1 = ((bf16[32,12,256]{2,1,0:T(8,128)(2,1)}), bf16[32,12,256]{2,1,0:T(8,128)(2,1)S(1)}, u32[]{:S(2)}, u32[]{:S(2)}) async-start(bf16[32,12,256]{2,1,0:T(8,128)(2,1)} %reshape.50), calls=%async_computation.2 | async-start | bytes 524288 | tf_op jit(solution)/shard_map/all_to_all | solution.py:90
Sparse Core Ops, SparseCore 0:
  35.7 43.5 all-gather.1
  103.3 64.4 reduce-scatter.1
where the time goes:
time: 200 us; the launch traced here: 199 us
  waiting for transfers between devices  117 us (58%)
  blocking collectives  22.7 us (11%)
  local copies, waits for them, and re-layouts  15.3 us (8%)
  between operations  13.6 us (7%)
  matrix products  12.3 us (6%)
  starting transfers between devices  9.94 us (5%)
  other arithmetic  7.8 us (4%)
    reduce_scatter x1, waiting for transfers between devices, in_one_piece(): filled = lax.psum_scatter(both, axis, scatter_dimension=dim, tiled=True)  64.6 us
    all_gather x1, waiting for transfers between devices, body(): piece = lax.all_gather(arrived, 'tp', axis=3, tiled=True)  41.6 us
    all_to_all x1, blocking collectives, body(): lax.all_to_all(buffer, 'ep', split_axis=0, concat_axis=0, tiled=True)  22.7 us
    all_to_all x1, waiting for transfers between devices, body(): lax.all_to_all(expert_out, 'ep', split_axis=0, concat_axis=0, tiled=True)  11.1 us
    all_to_all x1, starting transfers between devices, body(): lax.all_to_all(expert_out, 'ep', split_axis=0, concat_axis=0, tiled=True)  9.9 us
    convert_element_type x1, local copies, waits for them, and re-layouts, body(): partial_value.reshape(-1, width).astype(jnp.bfloat16)  5.73 us
    dot_general x1, matrix products, body(): jnp.einsum('secf,efd->secd', hidden, expert_down, preferred_element_type=...  5.72 us
    optimization_barrier x1, local copies, waits for them, and re-layouts, rounded(): lax.optimization_barrier(values.astype(jnp.bfloat16)).astype(jnp.float32)  5.57 us
  transfers between devices with their start and end apart: 3, of which 3 were waited for; matrix products, arithmetic and copies ran while one was open for 1% of the time, Pallas kernels for 0%

commit v1 on v0

--- a/solution.py
+++ b/solution.py
@@ -60,7 +60,9 @@
     buffer = jnp.dot(table, own_cols, preferred_element_type=jnp.float32).astype(jnp.bfloat16)
     buffer = buffer.reshape(ep_size, local, slot_count, columns)
     arrived = lax.all_to_all(buffer, "ep", split_axis=0, concat_axis=0, tiled=True)
-    piece = lax.all_gather(arrived, "tp", axis=3, tiled=True)
+    piece = jnp.concatenate(
+        lax.all_to_all(jnp.stack([arrived] * lax.axis_size("tp")), "tp", 0, 0), axis=3
+    )
     gate = jnp.einsum("secd,efd->secf", piece, expert_gate, preferred_element_type=jnp.float32)
     upper = jnp.einsum("secd,efd->secf", piece, expert_up, preferred_element_type=jnp.float32)
     gate, upper = (gate, upper)

time: 200 us -> 233 us (1.17)
  waiting for transfers between devices: 117 us -> 139 us
  starting transfers between devices: 9.94 us -> 19.6 us
  local copies, waits for them, and re-layouts: 15.3 us -> 20.7 us
  matrix products: 12.3 us -> 8.92 us
    all_to_all x0 -> x1, waiting for transfers between devices: none -> 70.3 us  [body(): lax.all_to_all(jnp.stack([arrived] * lax.axis_size('tp')), 'tp', 0, 0)]
    all_gather x1 -> x0, waiting for transfers between devices: 41.6 us -> none  [body(): piece = lax.all_gather(arrived, 'tp', axis=3, tiled=True)]
    all_to_all x0 -> x1, starting transfers between devices: none -> 9.7 us  [body(): lax.all_to_all(jnp.stack([arrived] * lax.axis_size('tp')), 'tp', 0, 0)]
    reduce_scatter x1, waiting for transfers between devices: 64.6 us -> 57.5 us  [in_one_piece(): filled = lax.psum_scatter(both, axis, scatter_dimension=dim, tiled=True)]
    reshape x0 -> x1, local copies, waits for them, and re-layouts: none -> 2.37 us  [body(): jnp.concatenate(lax.all_to_all(jnp.stack([arrived] * lax.axis_size('tp'))...]
  transfers between devices with their start and end apart: 3 -> 3, of which waited for: 3 -> 3; matrix products, arithmetic and copies ran while one was open for 1% -> 0% of each run, Pallas kernels for 0% -> 0%
where the time goes in v1:
time: 233 us; the launch traced here: 232 us
  waiting for transfers between devices  139 us (60%)
  blocking collectives  22.7 us (10%)
  local copies, waits for them, and re-layouts  20.7 us (9%)
  starting transfers between devices  19.6 us (8%)
  between operations  13.6 us (6%)
  matrix products  8.92 us (4%)
  other arithmetic  7.8 us (3%)
    all_to_all x1, waiting for transfers between devices, body(): lax.all_to_all(jnp.stack([arrived] * lax.axis_size('tp')), 'tp', 0, 0)  70.3 us
    reduce_scatter x1, waiting for transfers between devices, in_one_piece(): filled = lax.psum_scatter(both, axis, scatter_dimension=dim, tiled=True)  57.5 us
    all_to_all x1, blocking collectives, body(): lax.all_to_all(buffer, 'ep', split_axis=0, concat_axis=0, tiled=True)  22.7 us
    all_to_all x1, waiting for transfers between devices, body(): lax.all_to_all(expert_out, 'ep', split_axis=0, concat_axis=0, tiled=True)  11.1 us
    all_to_all x1, starting transfers between devices, body(): lax.all_to_all(expert_out, 'ep', split_axis=0, concat_axis=0, tiled=True)  9.89 us
    all_to_all x1, starting transfers between devices, body(): lax.all_to_all(jnp.stack([arrived] * lax.axis_size('tp')), 'tp', 0, 0)  9.7 us
    convert_element_type x1, local copies, waits for them, and re-layouts, body(): partial_value.reshape(-1, width).astype(jnp.bfloat16)  5.73 us
    optimization_barrier x1, local copies, waits for them, and re-layouts, rounded(): lax.optimization_barrier(values.astype(jnp.bfloat16)).astype(jnp.float32)  5.57 us
  transfers between devices with their start and end apart: 3, of which 3 were waited for; matrix products, arithmetic and copies ran while one was open for 0% of the time, Pallas kernels for 0%

profile of v1, /device:TPU:25, one launch (start us, length us, event | category | flops | bytes accessed | tf_op | source)
XLA Modules:
  0.0 232.3 jit_solution(1607759236930833635)
XLA Ops:
  6.5 0.9 copy.41
  7.4 0.1 eq.48
  7.5 0.6 reduce-window.6
  8.1 0.2 slice_reduce_fusion
  8.4 0.1 bitcast_bitcast_fusion
  8.5 0.1 reduce_sum.48
  8.7 0.7 multiply_add_fusion
  9.4 0.1 convert_reduce_fusion
  9.5 1.1 fusion.9
  10.6 1.1 fusion.11
  11.6 0.2 convolution_convert_fusion.2
  12.0 0.2 copy.45
  12.1 22.7 %all_to_all.15 = bf16[32,2,6,256]{3,1,2,0:T(2,128)(2,1)S(1)} all-to-all(bf16[32,2,6,256]{3,1,2,0:T(2,128)(2,1)S(1)} %copy.45), channel_id=1, replica_groups=mesh['ep'=32,'tp'=16] {'ep'}, dimensions={0} | all-to-all | bytes 393216 | tf_op jit(solution)/shard_map/all_to_all | solution.py:62
  34.8 2.1 stack.2
  36.9 9.7 %all-to-all-start.1 = ((bf16[16,32,2,6,256]{4,1,3,2,0:T(8,128)(2,1)}), bf16[16,32,2,6,256]{4,1,3,2,0:T(8,128)(2,1)}, u32[]{:S(2)}, u32[]{:S(2)}) async-start(bf16[16,32,2,6,256]{4,1,3,2,0:T(8,128)(2,1)} %stack.2), calls=%async_computation.1 | async-start | bytes 6291456 | tf_op jit(solution)/shard_map/all_to_all | solution.py:64
  46.7 0.2 fusion.31
  46.9 0.6 convolution_convert_fusion.1
  47.5 70.3 %all-to-all-done.1 = bf16[16,32,2,6,256]{4,1,3,2,0:T(8,128)(2,1)} async-done(((bf16[16,32,2,6,256]{4,1,3,2,0:T(8,128)(2,1)}), bf16[16,32,2,6,256]{4,1,3,2,0:T(8,128)(2,1)}, u32[]{:S(2)}, u32[]{:S(2)}) %all-to-all-start.1) | async-done | bytes 3145760 | tf_op jit(solution)/shard_map/all_to_all | solution.py:64
  117.9 2.4 %copy.54 = bf16[16,2,6,4,8,256]{5,4,0,3,2,1:T(8,128)(2,1)S(1)} copy(bf16[16,2,6,4,8,256]{5,4,3,2,1,0:T(8,128)(2,1)} %bitcast.18) | data formatting | bytes 6291456 | tf_op jit(solution)/shard_map/reshape | solution.py:63
  120.3 1.7 copy-done.1
  121.9 1.0 convolution_bitcast_fusion.1
  122.9 5.4 %fusion = bf16[32,2,6,4096]{3,0,2,1:T(8,128)(2,1)} fusion(bf16[32,2,6,4096]{3,0,2,1:T(8,128)(2,1)} %bitcast.54, bf16[2,64,4096]{2,1,0:T(8,128)(2,1)S(1)} %copy-done, bf16[2,64,4096]{2,1,0:T(8,128)(2,1)S(1)} %copy-done.3, f32[32,2,6,64]{3,0,2,1:T(8,128)S(1)} %convolution_bitcast_fusion.1), kind=kOutput, calls=%fused_computation.1 | convolution fusion | flops 404373504 | bytes 8486912 | tf_op jit(solution)/shard_map/secf,efd->secd/dot_general | solution.py:71
  128.3 5.6 %copy.48 = bf16[32,2,6,4096]{3,2,1,0:T(8,128)(2,1)} copy(bf16[32,2,6,4096]{3,0,2,1:T(8,128)(2,1)} %fusion) | data formatting | bytes 6291456 | tf_op jit(solution)/shard_map/optimization_barrier | solution.py:27
  133.9 5.7 %convert_element_type.60 = bf16[384,4096]{1,0:T(8,128)(2,1)} reshape(bf16[32,2,6,4096]{3,2,1,0:T(8,128)(2,1)} %copy.48) | data formatting | bytes 6291456 | tf_op jit(solution)/shard_map/convert_element_type | solution.py:82
  139.6 3.9 %pad_maximum_fusion = bf16[408,4096]{1,0:T(8,128)(2,1)} fusion(bf16[24,4096]{1,0:T(8,128)(2,1)S(1)} %convolution_convert_fusion.1, bf16[384,4096]{1,0:T(8,128)(2,1)} %convert_element_type.60), kind=kLoop, calls=%fused_computation.3 | loop fusion | flops 6684672 | bytes 6684672 | tf_op jit(solution)/shard_map/concatenate | solution.py:9
  143.6 57.5 %reduce-scatter.2.cloned.1.call-done = bf16[408,256]{1,0:T(8,128)(2,1)} async-done(((bf16[408,4096]{1,0:T(8,128)(2,1)}), bf16[408,256]{1,0:T(8,128)(2,1)}) %reduce-scatter.2.cloned.1.call-update) | async-done | bytes 208912 | tf_op jit(solution)/shard_map/reduce_scatter | solution.py:10
  201.1 0.9 split.9
  202.1 0.7 reshape.60
  202.8 9.9 %all-to-all-start.2 = ((bf16[32,12,256]{2,1,0:T(8,128)(2,1)}), bf16[32,12,256]{2,1,0:T(8,128)(2,1)S(1)}, u32[]{:S(2)}, u32[]{:S(2)}) async-start(bf16[32,12,256]{2,1,0:T(8,128)(2,1)} %reshape.60), calls=%async_computation.3 | async-start | bytes 524288 | tf_op jit(solution)/shard_map/all_to_all | solution.py:92
  212.8 0.1 select_reduce_fusion
  212.9 11.1 %all-to-all-done.2 = bf16[32,12,256]{2,1,0:T(8,128)(2,1)S(1)} async-done(((bf16[32,12,256]{2,1,0:T(8,128)(2,1)}), bf16[32,12,256]{2,1,0:T(8,128)(2,1)S(1)}, u32[]{:S(2)}, u32[]{:S(2)}) %all-to-all-start.2) | async-done | bytes 196640 | tf_op jit(solution)/shard_map/all_to_all | solution.py:92
  224.0 1.5 fusion.3
  (29 shorter events, 0.4 us)
Async XLA Ops:
  6.5 116.4 %copy-start = (bf16[2,64,4096]{2,1,0:T(8,128)(2,1)S(1)}, bf16[2,64,4096]{2,1,0:T(8,128)(2,1)}, u32[]{:S(2)}) copy-start(bf16[2,64,4096]{2,1,0:T(8,128)(2,1)} %param.16) | copy-start | bytes 3145732
  36.9 9.8 %copy-start.4 = (bf16[64,4096]{1,0:T(8,128)(2,1)S(1)}, bf16[64,4096]{1,0:T(8,128)(2,1)}, u32[]{:S(2)}) copy-start(bf16[64,4096]{1,0:T(8,128)(2,1)} %param.17) | copy-start | bytes 1572868
  36.9 10.0 %copy-start.5 = (bf16[64,4096]{1,0:T(8,128)(2,1)S(1)}, bf16[64,4096]{1,0:T(8,128)(2,1)}, u32[]{:S(2)}) copy-start(bf16[64,4096]{1,0:T(8,128)(2,1)} %param.19) | copy-start | bytes 1572868
  36.9 10.0 %copy-start.6 = (bf16[64,4096]{1,0:T(8,128)(2,1)S(1)}, bf16[64,4096]{1,0:T(8,128)(2,1)}, u32[]{:S(2)}) copy-start(bf16[64,4096]{1,0:T(8,128)(2,1)} %param.18) | copy-start | bytes 1572868
  36.9 81.0 %all-to-all-start.1 = ((bf16[16,32,2,6,256]{4,1,3,2,0:T(8,128)(2,1)}), bf16[16,32,2,6,256]{4,1,3,2,0:T(8,128)(2,1)}, u32[]{:S(2)}, u32[]{:S(2)}) async-start(bf16[16,32,2,6,256]{4,1,3,2,0:T(8,128)(2,1)} %stack.2), calls=%async_computation.1 | async-start | bytes 6291456 | tf_op jit(solution)/shard_map/all_to_all | solution.py:64
  46.6 154.5 %reduce-scatter.2.cloned.1.call-start = ((), (), s32[]{:S(2)}) async-start(), calls=%async_computation.4 | async-start | bytes 3551232 | tf_op jit(solution)/shard_map/reduce_scatter | solution.py:10
  117.9 4.1 %copy-start.2 = (bf16[2,64,4096]{2,1,0:T(8,128)(2,1)S(1)}, bf16[2,64,4096]{2,1,0:T(8,128)(2,1)}, u32[]{:S(2)}) copy-start(bf16[2,64,4096]{2,1,0:T(8,128)(2,1)} %param.14) | copy-start | bytes 3145732
  120.2 1.7 copy-start.1
  120.3 2.6 %copy-start.3 = (bf16[2,64,4096]{2,1,0:T(8,128)(2,1)S(1)}, bf16[2,64,4096]{2,1,0:T(8,128)(2,1)}, u32[]{:S(2)}) copy-start(bf16[2,64,4096]{2,1,0:T(8,128)(2,1)} %param.15) | copy-start | bytes 3145732
  143.6 69.1 %copy-start.7 = (f32[24,6]{0,1:T(8,128)S(1)}, f32[24,6]{0,1:T(8,128)}, u32[]{:S(2)}) copy-start(f32[24,6]{0,1:T(8,128)} %param.13) | copy-start | bytes 1732
  202.8 21.1 %all-to-all-start.2 = ((bf16[32,12,256]{2,1,0:T(8,128)(2,1)}), bf16[32,12,256]{2,1,0:T(8,128)(2,1)S(1)}, u32[]{:S(2)}, u32[]{:S(2)}) async-start(bf16[32,12,256]{2,1,0:T(8,128)(2,1)} %reshape.60), calls=%async_computation.3 | async-start | bytes 524288 | tf_op jit(solution)/shard_map/all_to_all | solution.py:92
Sparse Core Ops, SparseCore 0:
  143.7 57.3 reduce-scatter.1
